TPU v7x, 512 devices: a 4x2x32 block of a 4x8x32 slice. The times are simulated.
512 devices in a mesh: grp: 2 (over y), sp: 64 (over z, core), tp: 4 (over x).
Axes of the slice: x: 4, y: 2, z: 32, core: 2. Of those that a mesh axis runs over, the one named last changes fastest.
The devices are a block of a 4x8x32 slice.
Arguments:
- tokens: bfloat16 [65536, 2048], P(('grp', 'sp')), parts along dimension 0, may hold values from -6 to 6
- gate_in: bfloat16 [2, 2048, 512], P(None, 'sp', 'tp'), may hold values from -0.125 to 0.125
- gate_conv: bfloat16 [2, 2048, 512], P(None, 'sp', 'tp'), may hold values from -0.125 to 0.125
- value_in: bfloat16 [2, 2048, 512], P(None, 'sp', 'tp'), may hold values from -0.125 to 0.125
- out_weight: bfloat16 [2, 512, 2048], P(None, None, 'sp'), may hold values from -0.25 to 0.25
- conv_taps: float32 [2, 3, 512], replicated, may hold values from -7 to 7
- pre_gain: float32 [2, 2048], replicated, may hold values from 0.1 to 1.9
- mix_gain: float32 [2, 512], replicated, may hold values from 0.1 to 1.9
- post_gain: float32 [2, 2048], replicated, may hold values from 0.1 to 1.9
Outputs:
- result: bfloat16 [65536, 2048], P(('grp', 'sp', 'tp')), parts along dimension 0
There are 2 independent parts, one for each index of `grp`. A program takes and returns all parts, laid end to end along the dimension named above; an argument that names none is the same for every part. Nothing has to cross between parts.
All inputs are finite; a program needn't handle non-finite values.
Results may differ from a plain program's by a relative error of at most 0.011.
Values may be sent and summed in bfloat16 or wider, within the bound.
No kernel may reach another device: no remote copies, remote signals or barrier semaphores. Data moves between devices by JAX's collectives and lax.ppermute only.
A program may use at most 64 MiB of HBM per device.

v0:
```python
import jax
import jax.numpy as jnp
from jax import lax
from jax.sharding import PartitionSpec as P

EPS = 1e-06


def rows_first(arrays, axis, dims):
    turned = [jnp.moveaxis(a, dim, 0) for a, dim in zip(arrays, dims)]
    widths = [t[0].size for t in turned]
    both = jnp.concatenate([t.reshape(-1, w) for t, w in zip(turned, widths)], axis=1)
    whole = lax.all_gather(both, axis, axis=0, tiled=True)
    tiles = jnp.split(whole, [sum(widths[:k]) for k in range(1, len(widths))], axis=1)
    return tuple(
        (
            jnp.moveaxis(b.reshape(-1, *t.shape[1:]), 0, dim)
            for b, t, dim in zip(tiles, turned, dims)
        )
    )


def passed_along(x, axis, by):
    length = lax.axis_size(axis)
    pairs = [(i, i + by) for i in range(length) if 0 <= i + by < length]
    return lax.ppermute(x, axis, pairs)


def in_order(tiles, dim):
    shape = list(tiles.shape[1:])
    shape[dim] *= tiles.shape[0]
    return jnp.moveaxis(tiles, 0, dim).reshape(shape)


def copy_for_each(x, axis):
    length = lax.axis_size(axis)
    return lax.all_to_all(jnp.broadcast_to(x[None], (length, *x.shape)), axis, 0, 0, tiled=True)


def gather_directly(x, axis, dim):
    return in_order(copy_for_each(x, axis), dim)


def rms_norm(values, gain):
    return values * lax.rsqrt(jnp.mean(values * values, axis=-1, keepdims=True) + EPS) * gain


def stored(values):
    return lax.optimization_barrier(values.astype(jnp.bfloat16))


def per_device(
    tokens, gate_in, gate_conv, value_in, out_weight, conv_taps, pre_gain, mix_gain, post_gain
):
    layer_count = gate_in.shape[0]
    channel_count = gate_in.shape[2]
    tap_count = conv_taps.shape[1]
    row_count = tokens.shape[0]
    tp_size = lax.axis_size("tp")
    tp_index = lax.axis_index("tp")
    row_share = row_count // tp_size
    all_outer, all_inner, all_values, all_out = rows_first(
        (gate_in, gate_conv, value_in, out_weight), "sp", (1, 1, 1, 2)
    )
    stream = tokens.astype(jnp.float32)
    for layer_index in range(layer_count):
        is_last = layer_index == layer_count - 1
        normed = stored(rms_norm(stream, pre_gain[layer_index]))
        outer_whole = all_outer[layer_index]
        inner_whole = all_inner[layer_index]
        value_whole = all_values[layer_index]
        out_whole = all_out[layer_index]
        outer = stored(jnp.dot(normed, outer_whole, preferred_element_type=jnp.float32))
        inner = stored(jnp.dot(normed, inner_whole, preferred_element_type=jnp.float32))
        values = stored(jnp.dot(normed, value_whole, preferred_element_type=jnp.float32))
        gated = stored(inner.astype(jnp.float32) * values.astype(jnp.float32))
        before = passed_along(gated[row_count - (tap_count - 1) :], "sp", 1)
        padded = jnp.concatenate([before, gated], axis=0)
        taps_here = lax.dynamic_slice_in_dim(
            conv_taps[layer_index], tp_index * channel_count, channel_count, 1
        )
        filtered = jnp.zeros((row_count, channel_count), jnp.float32)
        for tap_index in range(tap_count):
            filtered = filtered + taps_here[tap_index] * padded[
                tap_index : tap_index + row_count
            ].astype(jnp.float32)
        mixed_raw = stored(outer.astype(jnp.float32) * filtered)
        if is_last:
            arrived = lax.all_to_all(mixed_raw, "tp", split_axis=0, concat_axis=1, tiled=True)
            residual = lax.dynamic_slice_in_dim(stream, tp_index * row_share, row_share, 0)
        else:
            arrived = gather_directly(mixed_raw, "tp", 1)
            residual = stream
        mixed = stored(rms_norm(arrived.astype(jnp.float32), mix_gain[layer_index]))
        branch = stored(jnp.dot(mixed, out_whole, preferred_element_type=jnp.float32))
        stream = residual + rms_norm(branch.astype(jnp.float32), post_gain[layer_index])
    return stream.astype(jnp.bfloat16)


def solution(mesh):
    placed = (
        P(("grp", "sp"), None),
        P(None, "sp", "tp"),
        P(None, "sp", "tp"),
        P(None, "sp", "tp"),
        P(None, None, "sp"),
        P(),
        P(),
        P(),
        P(),
    )
    return jax.shard_map(
        per_device,
        mesh=mesh,
        in_specs=placed,
        out_specs=P(("grp", "sp", "tp"), None),
        check_vma=False,
    )
```

profile of v0, /device:TPU:40, one launch (start us, length us, event | category | flops | bytes accessed | tf_op | source)
XLA Modules:
  0.0 234.2 jit_solution(8318668567519101586)
XLA Ops:
  6.6 1.0 copy.27
  7.6 0.7 copy_bitcast_fusion.2
  8.3 0.7 copy_bitcast_fusion
  9.7 2.1 fusion.2
  11.9 1.9 fusion.4
  13.9 160.3 %all-gather.2.cloned.1.call-done = bf16[2048,1792]{1,0:T(8,128)(2,1)} async-done(((bf16[32,1792]{1,0:T(8,128)(2,1)}), bf16[2048,1792]{1,0:T(8,128)(2,1)}) %all-gather.2.cloned.1.call-update) | async-done | bytes 7340048 | tf_op jit(solution)/shard_map/all_gather | solution.py:13
  174.2 2.4 %slice_bitcast_fusion.6 = (bf16[256,2,8,128]{3,2,1,0:T(8,128)(2,1)S(1)}, bf16[256,2,8,128]{3,2,1,0:T(8,128)(2,1)S(1)}, bf16[256,2,8,128]{3,2,1,0:T(8,128)(2,1)S(1)}) fusion(bf16[2048,1792]{1,0:T(8,128)(2,1)} %all-gather.2.cloned.1.call-done), kind=kLoop, calls=%fused_computation.33 | loop fusion | bytes 6291456
  176.7 1.9 copy-done.3
  178.6 0.7 convolution_convert_fusion.6
  179.4 0.7 convolution_convert_fusion.5
  180.2 2.2 collective-permute-start
  182.5 0.7 convolution_convert_fusion.7
  183.7 0.8 broadcast_in_dim.2
  184.5 4.3 %all-to-all-start = ((bf16[4,512,128]{1,2,0:T(8,128)(2,1)}), bf16[4,512,128]{1,2,0:T(8,128)(2,1)S(1)}, u32[]{:S(2)}, u32[]{:S(2)}) async-start(bf16[4,512,128]{1,2,0:T(8,128)(2,1)} %broadcast_in_dim.2), calls=%async_computation | async-start | bytes 1048576 | tf_op jit(solution)/shard_map/all_to_all | solution.py:37
  188.8 4.7 %split.19 = bf16[2048,1024]{1,0:T(8,128)(2,1)} slice(bf16[2048,1792]{1,0:T(8,128)(2,1)} %all-gather.2.cloned.1.call-done), slice={[0:2048], [768:1792]} | slice | bytes 8388608 | tf_op jit(solution)/shard_map/split | solution.py:14
  193.5 6.5 %copy.20 = bf16[2048,1024]{0,1:T(8,128)(2,1)} copy(bf16[2048,1024]{1,0:T(8,128)(2,1)} %split.19) | data formatting | bytes 8388608 | tf_op jit(solution)/shard_map/reshape | solution.py:17
  200.3 2.9 %convolution_convert_fusion = bf16[512,2048]{1,0:T(8,128)(2,1)S(1)} fusion(bf16[512,512]{0,1:T(8,128)(2,1)S(1)} %fusion.10, bf16[2,512,2048]{2,1,0:T(8,128)(2,1)} %bitcast.115), kind=kOutput, calls=%fused_computation.12 | convolution fusion | flops 1074790400 | bytes 4718592 | tf_op jit(solution)/shard_map/dot_general | solution.py:95
  203.7 1.1 multiply_reduce_fusion
  205.3 1.5 copy-done.1
  208.8 2.4 %collective-permute-start.1 = (bf16[2,128]{1,0:T(2,128)(2,1)S(1)}, bf16[2,128]{1,0:T(2,128)(2,1)S(1)}, u32[]{:S(2)}, u32[]{:S(2)}) collective-permute-start(bf16[2,128]{1,0:T(2,128)(2,1)S(1)} %slice.128), channel_id=1, source_target_pairs={{0,4},{4,8},{8,12},{12,16},{16,20},{20,24},{24,28},{28,32},{32,36}... | collective-permute-start | bytes 1544 | tf_op jit(solution)/shard_map/ppermute | solution.py:26
  211.2 0.7 convolution_convert_fusion.4
  212.3 10.3 %all_to_all.18 = bf16[4,128,128]{1,2,0:T(8,128)(2,1)S(1)} all-to-all(bf16[4,128,128]{1,2,0:T(8,128)(2,1)S(1)} %copy.19), channel_id=1, replica_groups=mesh['grp'=2,'sp'=64,'tp'=4] {'tp'}, dimensions={0} | all-to-all | bytes 262144 | tf_op jit(solution)/shard_map/all_to_all | solution.py:89
  222.8 2.1 convolution_convert_fusion.1
  225.1 2.3 fusion.8
  (64 shorter events, 5.6 us)
Async XLA Ops:
  6.5 1.7 copy-start
  6.6 5.3 %copy-start.2 = (bf16[512,2048]{1,0:T(8,128)(2,1)S(1)}, bf16[512,2048]{1,0:T(8,128)(2,1)}, u32[]{:S(2)}) copy-start(bf16[512,2048]{1,0:T(8,128)(2,1)} %param.9) | copy-start | bytes 6291460
  6.6 5.3 %copy-start.10 = (f32[2,2048]{1,0:T(2,128)S(1)}, f32[2,2048]{1,0:T(2,128)}, u32[]{:S(2)}) copy-start(f32[2,2048]{1,0:T(2,128)} %param.15) | copy-start | bytes 49156
  6.6 167.7 %all-gather.2.cloned.1.call-start = ((), (), s32[]{:S(2)}) async-start(), calls=%async_computation.2 | async-start | bytes 7454720 | tf_op jit(solution)/shard_map/all_gather | solution.py:13
  11.9 2.0 copy-start.12
  11.9 2.0 copy-start.13
  176.6 2.0 copy-start.3
  176.7 2.7 %copy-start.4 = (bf16[256,2,8,128]{3,2,0,1:T(8,128)(2,1)}, bf16[256,2,8,128]{3,2,0,1:T(8,128)(2,1)S(1)}, u32[]{:S(2)}) copy-start(bf16[256,2,8,128]{3,2,0,1:T(8,128)(2,1)S(1)} %copy.35) | copy-start | bytes 3145732
  179.4 3.0 %copy-start.6 = (bf16[256,2,8,128]{3,2,0,1:T(8,128)(2,1)}, bf16[256,2,8,128]{3,2,0,1:T(8,128)(2,1)S(1)}, u32[]{:S(2)}) copy-start(bf16[256,2,8,128]{3,2,0,1:T(8,128)(2,1)S(1)} %copy.34) | copy-start | bytes 3145732
  180.2 3.2 %collective-permute-start = (bf16[2,128]{1,0:T(2,128)(2,1)S(1)}, bf16[2,128]{1,0:T(2,128)(2,1)S(1)}, u32[]{:S(2)}, u32[]{:S(2)}) collective-permute-start(bf16[2,128]{1,0:T(2,128)(2,1)S(1)} %slice.121), channel_id=1, source_target_pairs={{0,4},{4,8},{8,12},{12,16},{16,20},{20,24},{24,28},{28,32},{32,36}... | collective-permute-start | bytes 1544 | tf_op jit(solution)/shard_map/ppermute | solution.py:26
  182.4 1.0 copy-start.8
  182.5 6.3 %copy-start.11 = (f32[2,2048]{1,0:T(2,128)S(1)}, f32[2,2048]{1,0:T(2,128)}, u32[]{:S(2)}) copy-start(f32[2,2048]{1,0:T(2,128)} %param.17) | copy-start | bytes 49156
  184.5 15.5 %all-to-all-start = ((bf16[4,512,128]{1,2,0:T(8,128)(2,1)}), bf16[4,512,128]{1,2,0:T(8,128)(2,1)S(1)}, u32[]{:S(2)}, u32[]{:S(2)}) async-start(bf16[4,512,128]{1,2,0:T(8,128)(2,1)} %broadcast_in_dim.2), calls=%async_computation | async-start | bytes 1048576 | tf_op jit(solution)/shard_map/all_to_all | solution.py:37
  204.8 2.0 copy-start.1
  204.8 2.0 copy-start.5
  206.8 1.2 copy-start.7
  208.1 3.1 %copy-start.9 = (bf16[256,2,8,128]{3,2,0,1:T(8,128)(2,1)S(1)}, bf16[256,2,8,128]{3,2,0,1:T(8,128)(2,1)}, u32[]{:S(2)}) copy-start(bf16[256,2,8,128]{3,2,0,1:T(8,128)(2,1)} %copy-done.8) | copy-start | bytes 3145732
  208.8 3.2 %collective-permute-start.1 = (bf16[2,128]{1,0:T(2,128)(2,1)S(1)}, bf16[2,128]{1,0:T(2,128)(2,1)S(1)}, u32[]{:S(2)}, u32[]{:S(2)}) collective-permute-start(bf16[2,128]{1,0:T(2,128)(2,1)S(1)} %slice.128), channel_id=1, source_target_pairs={{0,4},{4,8},{8,12},{12,16},{16,20},{20,24},{24,28},{28,32},{32,36}... | collective-permute-start | bytes 1544 | tf_op jit(solution)/shard_map/ppermute | solution.py:26
Sparse Core Ops, SparseCore 0:
  9.8 164.3 all-gather.1
where the time goes:
time: 237 us; the launch traced here: 234 us
  waiting for transfers between devices  160 us (68%)
  local copies, waits for them, and re-layouts  21.7 us (9%)
  between operations  13.8 us (6%)
  blocking collectives  10.3 us (4%)
  other arithmetic  9.99 us (4%)
  matrix products  9.18 us (4%)
  starting transfers between devices  8.78 us (4%)
    all_gather x1, waiting for transfers between devices, rows_first(): whole = lax.all_gather(both, axis, axis=0, tiled=True)  160 us
    all_to_all x1, blocking collectives, per_device(): lax.all_to_all(mixed_raw, 'tp', split_axis=0, concat_axis=1, tiled=True)  10.3 us
    reshape x4, local copies, waits for them, and re-layouts, rows_first(): b.reshape(-1, *t.shape[1:])  6.76 us
    unnamed x29, local copies, waits for them, and re-layouts  6.68 us
    dot_general x2, matrix products, per_device(): jnp.dot(mixed, out_whole, preferred_element_type=jnp.float32)  4.93 us
  transfers between devices with their start and end apart: 4, of which 2 were waited for; matrix products, arithmetic and copies ran while one was open for 7% of the time, Pallas kernels for 0%

commit v1 on v0

v1 whole, which is shorter than its diff:
```python
import jax
import jax.numpy as jnp
from jax import lax
from jax.sharding import PartitionSpec as P

EPS = 1e-06
GATE_SCALE = 2.0**18
OUT_SCALE = 2.0**17


def passed_along(x, axis, by):
    length = lax.axis_size(axis)
    pairs = [(i, i + by) for i in range(length) if 0 <= i + by < length]
    return lax.ppermute(x, axis, pairs)


def rms_norm(values, gain):
    return values * lax.rsqrt(jnp.mean(values * values, axis=-1, keepdims=True) + EPS) * gain


def stored(values):
    return lax.optimization_barrier(values.astype(jnp.bfloat16))


def sent(values, scale):
    return (values.astype(jnp.float32) * scale).astype(jnp.float16)


def received(values, scale):
    return stored(values.astype(jnp.float32) * (1.0 / scale))


def per_device(
    tokens, gate_in, gate_conv, value_in, out_weight, conv_taps, pre_gain, mix_gain, post_gain
):
    layer_count = gate_in.shape[0]
    channel_count = gate_in.shape[2]
    whole_count = out_weight.shape[1]
    tap_count = conv_taps.shape[1]
    row_count = tokens.shape[0]
    tp_size = lax.axis_size("tp")
    tp_index = lax.axis_index("tp")
    row_share = row_count // tp_size
    pieces = []
    for layer_index in range(layer_count):
        for w in (gate_in, gate_conv, value_in):
            pieces.append(sent(w[layer_index], GATE_SCALE))
        pieces.append(sent(out_weight[layer_index].T, OUT_SCALE))
    packed = jnp.concatenate(pieces, axis=1)
    whole = lax.all_gather(packed, "sp", axis=0, tiled=True)
    stream = tokens.astype(jnp.float32)
    start = 0
    for layer_index in range(layer_count):
        is_last = layer_index == layer_count - 1
        gates = received(whole[:, start : start + 3 * channel_count], GATE_SCALE)
        start += 3 * channel_count
        out_whole = received(whole[:, start : start + whole_count], OUT_SCALE)
        start += whole_count
        normed = stored(rms_norm(stream, pre_gain[layer_index]))
        mixers = stored(jnp.dot(normed, gates, preferred_element_type=jnp.float32))
        outer = mixers[:, :channel_count]
        inner = mixers[:, channel_count : 2 * channel_count]
        values = mixers[:, 2 * channel_count :]
        gated = stored(inner.astype(jnp.float32) * values.astype(jnp.float32))
        before = passed_along(gated[row_count - (tap_count - 1) :], "sp", 1)
        padded = jnp.concatenate([before, gated], axis=0)
        taps_here = lax.dynamic_slice_in_dim(
            conv_taps[layer_index], tp_index * channel_count, channel_count, 1
        )
        filtered = jnp.zeros((row_count, channel_count), jnp.float32)
        for tap_index in range(tap_count):
            filtered = filtered + taps_here[tap_index] * padded[
                tap_index : tap_index + row_count
            ].astype(jnp.float32)
        mixed_raw = stored(outer.astype(jnp.float32) * filtered)
        if is_last:
            arrived = lax.all_to_all(mixed_raw, "tp", split_axis=0, concat_axis=1, tiled=True)
            residual = lax.dynamic_slice_in_dim(stream, tp_index * row_share, row_share, 0)
        else:
            arrived = lax.all_gather(mixed_raw, "tp", axis=1, tiled=True)
            residual = stream
        mixed = stored(rms_norm(arrived.astype(jnp.float32), mix_gain[layer_index]))
        branch = stored(
            lax.dot_general(
                mixed, out_whole, (((1,), (1,)), ((), ())), preferred_element_type=jnp.float32
            )
        )
        stream = residual + rms_norm(branch.astype(jnp.float32), post_gain[layer_index])
    return stream.astype(jnp.bfloat16)


def solution(mesh):
    placed = (
        P(("grp", "sp"), None),
        P(None, "sp", "tp"),
        P(None, "sp", "tp"),
        P(None, "sp", "tp"),
        P(None, None, "sp"),
        P(),
        P(),
        P(),
        P(),
    )
    return jax.shard_map(
        per_device,
        mesh=mesh,
        in_specs=placed,
        out_specs=P(("grp", "sp", "tp"), None),
        check_vma=False,
    )
```

time: 237 us -> 176 us (0.74)
  waiting for transfers between devices: 160 us -> 7.13 us
  blocking collectives: 10.3 us -> 135 us
  local copies, waits for them, and re-layouts: 21.7 us -> 3.04 us
  between operations: 13.8 us -> 0.29 us
  other arithmetic: 9.99 us -> 17.1 us
  matrix products: 9.18 us -> 4.61 us
    all_gather x1 -> x0, waiting for transfers between devices: 160 us -> none  [rows_first(): whole = lax.all_gather(both, axis, axis=0, tiled=True)]
    all_gather x0 -> x2, blocking collectives: none -> 135 us  [the longest x1 120 us: per_device(): whole = lax.all_gather(packed, 'sp', axis=0, tiled=True)]
    all_to_all x1 -> x0, blocking collectives: 10.3 us -> none  [per_device(): lax.all_to_all(mixed_raw, 'tp', split_axis=0, concat_axis=1, tiled=True)]
    reshape x7 -> x0, local copies, waits for them, and re-layouts: 9.2 us -> none  [the longest x4 6.76 us: rows_first(): b.reshape(-1, *t.shape[1:])]
    all_to_all x1, waiting for transfers between devices: 0.01 us -> 6.35 us  [per_device(): lax.all_to_all(mixed_raw, 'tp', split_axis=0, concat_axis=1, tiled=True)]
    unnamed x0 -> x7, other arithmetic: none -> 5.02 us
    split x1 -> x0, local copies, waits for them, and re-layouts: 4.69 us -> none  [rows_first(): jnp.split(whole, [sum(widths[:k]) for k in range(1, len(widths))], axis=1)]
    dot_general x8 -> x4, matrix products: 9.18 us -> 4.61 us  [the longest x2 2.49 us: per_device(): mixers = stored(jnp.dot(normed, gates, preferred_element_type=jnp.float32))]
  transfers between devices with their start and end apart: 4 -> 3, of which waited for: 2 -> 2; matrix products, arithmetic and copies ran while one was open for 7% -> 2% of each run, Pallas kernels for 0% -> 0%
where the time goes in v1:
time: 176 us; the launch traced here: 174 us
  blocking collectives  135 us (77%)
  other arithmetic  17.1 us (10%)
  waiting for transfers between devices  7.13 us (4%)
  starting transfers between devices  7.02 us (4%)
  matrix products  4.61 us (3%)
  local copies, waits for them, and re-layouts  3.04 us (2%)
    all_gather x1, blocking collectives, per_device(): whole = lax.all_gather(packed, 'sp', axis=0, tiled=True)  120 us
    all_gather x1, blocking collectives, per_device(): arrived = lax.all_gather(mixed_raw, 'tp', axis=1, tiled=True)  15.2 us
    convert_element_type x10, other arithmetic, stored(): return lax.optimization_barrier(values.astype(jnp.bfloat16))  6.5 us
    all_to_all x1, waiting for transfers between devices, per_device(): lax.all_to_all(mixed_raw, 'tp', split_axis=0, concat_axis=1, tiled=True)  6.35 us
    unnamed x7, other arithmetic  5.02 us
    ppermute x2, starting transfers between devices, passed_along(): return lax.ppermute(x, axis, pairs)  3.6 us
  transfers between devices with their start and end apart: 3, of which 2 were waited for; matrix products, arithmetic and copies ran while one was open for 2% of the time, Pallas kernels for 0%

profile of v1, /device:TPU:40, one launch (start us, length us, event | category | flops | bytes accessed | tf_op | source)
XLA Modules:
  0.0 174.5 jit_solution(6006410904357195028)
XLA Ops:
  0.7 0.7 constant_dynamic-update-slice_fusion.4
  1.4 0.7 constant_dynamic-update-slice_fusion.3
  2.1 0.8 fusion.17
  2.9 0.7 constant_dynamic-update-slice_fusion.2
  3.6 0.7 constant_dynamic-update-slice_fusion.1
  4.3 0.7 constant_dynamic-update-slice_fusion
  5.0 0.8 fusion.19
  5.8 120.1 %all-gather.1 = f16[2048,1792]{1,0:T(8,128)(2,1)S(1)} all-gather(f16[32,1792]{1,0:T(8,128)(2,1)S(1)} %fusion.19), channel_id=1, replica_groups=mesh['grp'=2,'sp'=64,'tp'=4] {'sp'}, dimensions={0}, use_global_device_ids=true | all-gather | bytes 7454720 | tf_op jit(solution)/shard_map/all_gather | solution.py:50
  125.9 1.9 %multiply_convert_fusion.3 = (bf16[2048,384]{1,0:T(8,128)(2,1)}, bf16[2048,384]{1,0:T(8,128)(2,1)S(1)}) fusion(f16[2048,1792]{1,0:T(8,128)(2,1)S(1)} %all-gather.1), kind=kLoop, calls=%fused_computation.14 | loop fusion | flops 4718592 | bytes 6291456 | tf_op jit(solution)/shard_map/convert_element_type | solution.py:22
  128.9 1.2 convolution_convert_fusion.3
  130.2 2.3 %collective-permute-start = (bf16[2,128]{1,0:T(2,128)(2,1)S(1)}, bf16[2,128]{1,0:T(2,128)(2,1)S(1)}, u32[]{:S(2)}, u32[]{:S(2)}) collective-permute-start(bf16[2,128]{1,0:T(2,128)(2,1)S(1)} %slice.162), channel_id=1, source_target_pairs={{0,4},{4,8},{8,12},{12,16},{16,20},{20,24},{24,28},{28,32},{32,36}... | collective-permute-start | bytes 1544 | tf_op jit(solution)/shard_map/ppermute | solution.py:14
  132.5 3.0 %multiply_convert_fusion = (bf16[2048,512]{1,0:T(8,128)(2,1)}, bf16[2048,512]{1,0:T(8,128)(2,1)}) fusion(f16[2048,1792]{1,0:T(8,128)(2,1)S(1)} %all-gather.1), kind=kLoop, calls=%fused_computation.10 | loop fusion | flops 6291456 | bytes 8388608 | tf_op jit(solution)/shard_map/convert_element_type | solution.py:22
  135.8 15.2 %all_gather.7 = bf16[512,512]{1,0:T(8,128)(2,1)S(1)} all-gather(bf16[512,128]{1,0:T(8,128)(2,1)S(1)} %multiply_convert_fusion.7), channel_id=1, replica_groups=mesh['grp'=2,'sp'=64,'tp'=4] {'tp'}, dimensions={1}, use_global_device_ids=true | all-gather | bytes 655360 | tf_op jit(solution)/shard_map/all_gather | solution.py:80
  151.3 1.3 convolution_convert_fusion
  153.1 1.1 multiply_reduce_fusion
  154.7 1.5 copy-done
  156.8 1.2 convolution_convert_fusion.2
  158.2 1.3 collective-permute-start.1
  159.5 0.8 collective-permute-done.1
  160.4 0.8 copy.10
  161.2 3.4 %all-to-all-start = ((bf16[4,128,128]{1,2,0:T(8,128)(2,1)}), bf16[4,128,128]{1,2,0:T(8,128)(2,1)S(1)}, u32[]{:S(2)}, u32[]{:S(2)}) async-start(bf16[4,128,128]{1,2,0:T(8,128)(2,1)} %copy.10), calls=%async_computation | async-start | bytes 262144 | tf_op jit(solution)/shard_map/all_to_all | solution.py:77
  164.6 6.3 %all-to-all-done = bf16[4,128,128]{1,2,0:T(8,128)(2,1)S(1)} async-done(((bf16[4,128,128]{1,2,0:T(8,128)(2,1)}), bf16[4,128,128]{1,2,0:T(8,128)(2,1)S(1)}, u32[]{:S(2)}, u32[]{:S(2)}) %all-to-all-start) | async-done | bytes 131104 | tf_op jit(solution)/shard_map/all_to_all | solution.py:77
  171.2 0.8 convolution_convert_fusion.1
  172.2 2.2 %fusion.11 = bf16[128,2048]{1,0:T(8,128)(2,1)} fusion(bf16[128,2048]{1,0:T(8,128)(2,1)S(1)} %convolution_convert_fusion.1, f32[512,2048]{1,0:T(8,128)} %copy-done, s32[]{:T(128)S(6)} %select_n.2, f32[2048]{0:T(1024)S(1)} %bitcast.72, f32[128]{0:T(128)S(1)} %add_rsqrt_fusion.4), kind=kLoop, calls=%fused_computation.30 | loop fusion | flops 1310720 | bytes 2105860 | tf_op jit(solution)/shard_map/convert_element_type | solution.py:89
  (46 shorter events, 4.5 us)
Async XLA Ops:
  125.9 1.9 %copy-start.5 = (f32[2,2048]{1,0:T(2,128)S(1)}, f32[2,2048]{1,0:T(2,128)}, u32[]{:S(2)}) copy-start(f32[2,2048]{1,0:T(2,128)} %param.15) | copy-start | bytes 49156
  125.9 1.9 %copy-start.1 = (bf16[512,2048]{1,0:T(8,128)(2,1)S(1)}, bf16[512,2048]{1,0:T(8,128)(2,1)}, u32[]{:S(2)}) copy-start(bf16[512,2048]{1,0:T(8,128)(2,1)} %param.9) | copy-start | bytes 6291460
  130.2 5.4 %collective-permute-start = (bf16[2,128]{1,0:T(2,128)(2,1)S(1)}, bf16[2,128]{1,0:T(2,128)(2,1)S(1)}, u32[]{:S(2)}, u32[]{:S(2)}) collective-permute-start(bf16[2,128]{1,0:T(2,128)(2,1)S(1)} %slice.162), channel_id=1, source_target_pairs={{0,4},{4,8},{8,12},{12,16},{16,20},{20,24},{24,28},{28,32},{32,36}... | collective-permute-start | bytes 1544 | tf_op jit(solution)/shard_map/ppermute | solution.py:14
  132.5 3.0 %copy-start.7 = (f32[2,3,512]{2,0,1:T(2,128)S(1)}, f32[2,3,512]{2,0,1:T(2,128)}, u32[]{:S(2)}) copy-start(f32[2,3,512]{2,0,1:T(2,128)} %param.14) | copy-start | bytes 36868
  132.5 3.0 %copy-start.8 = (f32[2,512]{1,0:T(2,128)S(1)}, f32[2,512]{1,0:T(2,128)}, u32[]{:S(2)}) copy-start(f32[2,512]{1,0:T(2,128)} %param.16) | copy-start | bytes 12292
  132.5 3.0 %copy-start.6 = (f32[2,2048]{1,0:T(2,128)S(1)}, f32[2,2048]{1,0:T(2,128)}, u32[]{:S(2)}) copy-start(f32[2,2048]{1,0:T(2,128)} %param.17) | copy-start | bytes 49156
  135.6 15.7 %copy-start.3 = (bf16[2048,512]{1,0:T(8,128)(2,1)S(1)}, bf16[2048,512]{1,0:T(8,128)(2,1)}, u32[]{:S(2)}) copy-start(bf16[2048,512]{1,0:T(8,128)(2,1)} %get-tuple-element.8) | copy-start | bytes 6291460
  154.2 2.0 %copy-start = (f32[512,2048]{1,0:T(8,128)}, f32[512,2048]{1,0:T(8,128)S(1)}, u32[]{:S(2)}) copy-start(f32[512,2048]{1,0:T(8,128)S(1)} %get-tuple-element.6) | copy-start | bytes 12582916
  154.3 2.6 %copy-start.4 = (bf16[2048,384]{1,0:T(8,128)(2,1)S(1)}, bf16[2048,384]{1,0:T(8,128)(2,1)}, u32[]{:S(2)}) copy-start(bf16[2048,384]{1,0:T(8,128)(2,1)} %get-tuple-element.9) | copy-start | bytes 4718596
  156.8 14.3 %copy-start.2 = (bf16[2048,512]{1,0:T(8,128)(2,1)S(1)}, bf16[2048,512]{1,0:T(8,128)(2,1)}, u32[]{:S(2)}) copy-start(bf16[2048,512]{1,0:T(8,128)(2,1)} %get-tuple-element.7) | copy-start | bytes 6291460
  158.2 2.1 %collective-permute-start.1 = (bf16[2,128]{1,0:T(2,128)(2,1)S(1)}, bf16[2,128]{1,0:T(2,128)(2,1)S(1)}, u32[]{:S(2)}, u32[]{:S(2)}) collective-permute-start(bf16[2,128]{1,0:T(2,128)(2,1)S(1)} %slice.170), channel_id=1, source_target_pairs={{0,4},{4,8},{8,12},{12,16},{16,20},{20,24},{24,28},{28,32},{32,36}... | collective-permute-start | bytes 1544 | tf_op jit(solution)/shard_map/ppermute | solution.py:14
  161.2 9.8 %all-to-all-start = ((bf16[4,128,128]{1,2,0:T(8,128)(2,1)}), bf16[4,128,128]{1,2,0:T(8,128)(2,1)S(1)}, u32[]{:S(2)}, u32[]{:S(2)}) async-start(bf16[4,128,128]{1,2,0:T(8,128)(2,1)} %copy.10), calls=%async_computation | async-start | bytes 262144 | tf_op jit(solution)/shard_map/all_to_all | solution.py:77

commit v2 on v1

v2 whole, which is shorter than its diff:
```python
import jax
import jax.numpy as jnp
from jax import lax
from jax.experimental import pallas as pl
from jax.experimental.pallas import tpu as pltpu
from jax.sharding import PartitionSpec as P

EPS = 1e-06
GATE_SCALE = 2.0**18
OUT_SCALE = 2.0**17
HALO = 16
PAD = 8
BLOCK = 128
PARTS = 4

VMEM_LIMIT = 24 * 1024 * 1024


def scale_of(values, count):
    return lax.rsqrt(jnp.sum(values * values, axis=-1, keepdims=True) * (1.0 / count) + EPS)


def pack_kernel(gate_in, gate_conv, value_in, out_turned, tail, packed, tail_out):
    layers, _, channels = gate_in.shape
    whole = out_turned.shape[2]
    start = 0
    for layer in range(layers):
        for w in (gate_in, gate_conv, value_in):
            scaled = w[layer].astype(jnp.float32) * GATE_SCALE
            packed[:, start : start + channels] = scaled.astype(jnp.bfloat16)
            start += channels
        scaled = out_turned[layer].astype(jnp.float32) * OUT_SCALE
        packed[:, start : start + whole] = scaled.astype(jnp.bfloat16)
        start += whole
    tail_out[...] = tail[...]


def pack(tokens, gate_in, gate_conv, value_in, out_turned):
    rows = gate_in.shape[1]
    columns = gate_in.shape[0] * (3 * gate_in.shape[2] + out_turned.shape[2])
    count, width = tokens.shape
    return pl.pallas_call(
        pack_kernel,
        grid=(1,),
        in_specs=[
            pl.BlockSpec(gate_in.shape, lambda i: (0, 0, 0)),
            pl.BlockSpec(gate_in.shape, lambda i: (0, 0, 0)),
            pl.BlockSpec(gate_in.shape, lambda i: (0, 0, 0)),
            pl.BlockSpec(out_turned.shape, lambda i: (0, 0, 0)),
            pl.BlockSpec((HALO, width), lambda i: (count // HALO - 1, 0)),
        ],
        out_specs=[
            pl.BlockSpec((rows, columns), lambda i: (0, 0)),
            pl.BlockSpec((HALO, width), lambda i: (0, 0)),
        ],
        out_shape=[
            jax.ShapeDtypeStruct((rows, columns), jnp.bfloat16),
            jax.ShapeDtypeStruct((HALO, width), jnp.bfloat16),
        ],
        name="pack",
    )(gate_in, gate_conv, value_in, out_turned, tokens)


def in_blocks(rows):
    return [(0, HALO)] + [(HALO + start, BLOCK) for start in range(0, rows, BLOCK)]


def mix(normed, gates, taps, layer, tp_index, gated_rows, raw_of):
    rows = normed.shape[0]
    tap_count = taps.shape[1]
    channels = gates.shape[1] // 3
    mine = pl.ds(pl.multiple_of(tp_index * channels, channels), channels)
    mixers = jnp.dot(normed[...], gates[...], preferred_element_type=jnp.float32)
    mixers = mixers.astype(jnp.bfloat16).astype(jnp.float32)
    gated = mixers[:, channels : 2 * channels] * mixers[:, 2 * channels :]
    gated_rows[0:PAD, :] = jnp.zeros((PAD, channels), jnp.float32)
    gated_rows[PAD:, :] = gated.astype(jnp.bfloat16).astype(jnp.float32)
    filtered = None
    for tap in range(tap_count):
        at = PAD - (tap_count - 1) + tap
        term = taps[layer, tap : tap + 1, mine] * gated_rows[at : at + rows, :]
        filtered = term if filtered is None else filtered + term
    raw_of((mixers[:, :channels] * filtered).astype(jnp.bfloat16))


def first_kernel(
    tp_index, tokens, halo, gates, taps, pre_gain, raw, normed, gated_rows
):
    row_count, width = tokens.shape
    for first, count in in_blocks(row_count):
        rows = halo[...] if first == 0 else tokens[first - HALO : first - HALO + count, :]
        stream = rows.astype(jnp.float32)
        scale = scale_of(stream, width)
        normed[first : first + count, :] = (stream * scale * pre_gain[0:1, :]).astype(jnp.bfloat16)

    def store(values):
        for t in range(raw.shape[0]):
            raw[t] = values

    mix(normed, gates, taps, 0, tp_index[0], gated_rows, store)


def mixed_of(arrived, first, count, mix_gain, layer):
    parts = [arrived[t, first : first + count, :].astype(jnp.float32) for t in range(arrived.shape[0])]
    values = jnp.concatenate(parts, axis=1)
    return (values * scale_of(values, values.shape[1]) * mix_gain[layer : layer + 1, :]).astype(jnp.bfloat16)


def project(mixed, out_turned, branch):
    rows = out_turned.shape[0] // PARTS
    for part in range(PARTS):
        here = pl.ds(part * rows, rows)
        product = lax.dot_general(
            mixed, out_turned[here, :], (((1,), (1,)), ((), ())), preferred_element_type=jnp.float32
        )
        branch[:, here] = product.astype(jnp.bfloat16)


def added(stream, branch, post_gain, layer):
    branch = branch.astype(jnp.float32)
    return stream + branch * scale_of(branch, branch.shape[1]) * post_gain[layer : layer + 1, :]


def middle_kernel(
    tp_index, arrived, out_turned, tokens, halo, gates, taps, mix_gain, post_gain, pre_gain,
    raw, residual, mixed, branch, gated_rows,
):
    row_count, width = tokens.shape
    for first, count in in_blocks(row_count):
        mixed[first : first + count, :] = mixed_of(arrived, first, count, mix_gain, 0)
    project(mixed[...], out_turned, branch)
    for first, count in in_blocks(row_count):
        rows = halo[...] if first == 0 else tokens[first - HALO : first - HALO + count, :]
        stream = added(rows.astype(jnp.float32), branch[first : first + count, :], post_gain, 0)
        if first > 0:

            @pl.when(tp_index[0] == (first - HALO) // BLOCK)
            def _():
                residual[...] = stream

        scale = scale_of(stream, width)
        branch[first : first + count, :] = (stream * scale * pre_gain[1:2, :]).astype(jnp.bfloat16)

    def store(values):
        raw[...] = values[HALO:, :]

    mix(branch, gates, taps, 1, tp_index[0], gated_rows, store)


def last_kernel(arrived, out_turned, residual, mix_gain, post_gain, result, branch):
    mixed = mixed_of(arrived, 0, arrived.shape[1], mix_gain, 1)
    project(mixed, out_turned, branch)
    result[...] = added(residual[...], branch[...], post_gain, 1).astype(jnp.bfloat16)


def cost(rows, depth, columns):
    return pl.CostEstimate(flops=2 * rows * depth * columns, bytes_accessed=4 << 20, transcendentals=0)


def per_device(
    tokens, gate_in, gate_conv, value_in, out_weight, conv_taps, pre_gain, mix_gain, post_gain
):
    channels = gate_in.shape[2]
    whole = out_weight.shape[1]
    row_count, width = tokens.shape
    all_rows = HALO + row_count
    tp_size = lax.axis_size("tp")
    sp_size = lax.axis_size("sp")
    tp_index = lax.axis_index("tp")
    share = row_count // tp_size
    params = pltpu.CompilerParams(vmem_limit_bytes=VMEM_LIMIT)
    smem = pl.BlockSpec(memory_space=pltpu.SMEM)
    vmem = pl.BlockSpec(memory_space=pltpu.VMEM)

    packed, tail = pack(tokens, gate_in, gate_conv, value_in, jnp.swapaxes(out_weight, 1, 2))
    halo = lax.ppermute(tail, "sp", [(i, i + 1) for i in range(sp_size - 1)])
    gathered = lax.all_gather(packed.astype(jnp.float16), "sp", axis=0, tiled=True)
    stride = 3 * channels + whole

    def received(start, count, unscale):
        part = gathered[:, start : start + count].astype(jnp.float32) * unscale
        return part.astype(jnp.bfloat16)

    gates = [received(layer * stride, 3 * channels, 1.0 / GATE_SCALE) for layer in range(2)]
    gates, unscale = lax.optimization_barrier((gates, jnp.float32(1.0 / OUT_SCALE)))
    outs = [received(layer * stride + 3 * channels, whole, unscale) for layer in range(2)]
    gates, outs = lax.optimization_barrier((gates, outs))
    tp_index = tp_index.reshape(1)
    raw = pl.pallas_call(
        first_kernel,
        in_specs=[smem] + [vmem] * 5,
        out_specs=vmem,
        out_shape=jax.ShapeDtypeStruct((tp_size, all_rows, channels), jnp.bfloat16),
        scratch_shapes=[
            pltpu.VMEM((all_rows, width), jnp.bfloat16),
            pltpu.VMEM((PAD + all_rows, channels), jnp.float32),
        ],
        compiler_params=params,
        cost_estimate=cost(row_count, width, 3 * channels),
        name="first",
    )(tp_index, tokens, halo, gates[0], conv_taps, pre_gain)
    arrived = lax.all_to_all(raw, "tp", split_axis=0, concat_axis=0, tiled=True)
    raw, residual = pl.pallas_call(
        middle_kernel,
        in_specs=[smem] + [vmem] * 9,
        out_specs=[vmem, vmem],
        out_shape=[
            jax.ShapeDtypeStruct((row_count, channels), jnp.bfloat16),
            jax.ShapeDtypeStruct((share, width), jnp.float32),
        ],
        scratch_shapes=[
            pltpu.VMEM((all_rows, whole), jnp.bfloat16),
            pltpu.VMEM((all_rows, width), jnp.bfloat16),
            pltpu.VMEM((PAD + all_rows, channels), jnp.float32),
        ],
        compiler_params=params,
        cost_estimate=cost(row_count, width, 3 * channels + whole),
        name="middle",
    )(tp_index, arrived, outs[0], tokens, halo, gates[1], conv_taps, mix_gain, post_gain, pre_gain)
    arrived = lax.all_to_all(
        raw.reshape(tp_size, share, channels), "tp", split_axis=0, concat_axis=0, tiled=True
    )
    return pl.pallas_call(
        last_kernel,
        in_specs=[vmem] * 5,
        out_specs=vmem,
        out_shape=jax.ShapeDtypeStruct((share, width), jnp.bfloat16),
        scratch_shapes=[
            pltpu.VMEM((share, width), jnp.bfloat16),
        ],
        compiler_params=params,
        cost_estimate=cost(share, width, whole),
        name="last",
    )(arrived, outs[1], residual, mix_gain, post_gain)


def solution(mesh):
    placed = (
        P(("grp", "sp"), None),
        P(None, "sp", "tp"),
        P(None, "sp", "tp"),
        P(None, "sp", "tp"),
        P(None, None, "sp"),
        P(),
        P(),
        P(),
        P(),
    )
    return jax.shard_map(
        per_device,
        mesh=mesh,
        in_specs=placed,
        out_specs=P(("grp", "sp", "tp"), None),
        check_vma=False,
    )
```

time: 176 us -> 162 us (0.920)
  other arithmetic: 17.1 us -> 6.07 us
  Pallas kernels: 0 us -> 9.74 us
  waiting for transfers between devices: 7.13 us -> 0.01 us
  blocking collectives: 135 us -> 142 us
  starting transfers between devices: 7.02 us -> 1.83 us
  matrix products: 4.61 us -> 0 us
    all_to_all x0 -> x2, blocking collectives: none -> 23 us  [the longest x1 14.6 us: per_device(): arrived = lax.all_to_all(raw, 'tp', split_axis=0, concat_axis=0, tiled=True)]
    all_gather x2 -> x1, blocking collectives: 135 us -> 119 us  [per_device(): lax.all_gather(packed.astype(jnp.float16), 'sp', axis=0, tiled=True)]
    pallas_call x0 -> x4, Pallas kernels: none -> 9.74 us  [the longest x1 4.48 us: per_device(): pl.pallas_call(middle_kernel, in_specs=[smem] + [vmem] * 9, out_specs=[vm...]
    all_to_all x1 -> x0, waiting for transfers between devices: 6.35 us -> none  [per_device(): lax.all_to_all(mixed_raw, 'tp', split_axis=0, concat_axis=1, tiled=True)]
    unnamed x7 -> x0, other arithmetic: 5.02 us -> none
    dot_general x4 -> x0, matrix products: 4.61 us -> none  [the longest x2 2.49 us: per_device(): mixers = stored(jnp.dot(normed, gates, preferred_element_type=jnp.float32))]
    all_to_all x1 -> x0, starting transfers between devices: 3.42 us -> none  [per_device(): lax.all_to_all(mixed_raw, 'tp', split_axis=0, concat_axis=1, tiled=True)]
    convert_element_type x11 -> x3, other arithmetic: 8.74 us -> 6.07 us  [the longest x2 5.15 us: received(): return part.astype(jnp.bfloat16)]
  transfers between devices with their start and end apart: 3 -> 1, of which waited for: 2 -> 0; matrix products, arithmetic and copies ran while one was open for 2% -> 4% of each run, Pallas kernels for 0% -> 0%
where the time goes in v2:
time: 162 us; the launch traced here: 161 us
  blocking collectives  142 us (88%)
  Pallas kernels  9.74 us (6%)
  other arithmetic  6.07 us (4%)
  starting transfers between devices  1.83 us (1%)
    all_gather x1, blocking collectives, per_device(): lax.all_gather(packed.astype(jnp.float16), 'sp', axis=0, tiled=True)  119 us
    all_to_all x1, blocking collectives, per_device(): arrived = lax.all_to_all(raw, 'tp', split_axis=0, concat_axis=0, tiled=True)  14.6 us
    all_to_all x1, blocking collectives, per_device(): lax.all_to_all(raw.reshape(tp_size, share, channels), 'tp', split_axis=0,...  8.39 us
    convert_element_type x2, other arithmetic, received(): return part.astype(jnp.bfloat16)  5.15 us
    pallas_call x1, Pallas kernels, per_device(): pl.pallas_call(middle_kernel, in_specs=[smem] + [vmem] * 9, out_specs=[vm...  4.48 us
  transfers between devices with their start and end apart: 1, of which 0 were waited for; matrix products, arithmetic and copies ran while one was open for 4% of the time, Pallas kernels for 0%

profile of v2, /device:TPU:40, one launch (start us, length us, event | category | flops | bytes accessed | tf_op | source)
XLA Modules:
  0.0 161.4 jit_solution(2450576694880098687)
XLA Ops:
  0.0 1.6 pack.1
  1.6 1.8 %collective-permute-start = (bf16[16,2048]{1,0:T(8,128)(2,1)}, bf16[16,2048]{1,0:T(8,128)(2,1)S(1)}, u32[]{:S(2)}, u32[]{:S(2)}) collective-permute-start(bf16[16,2048]{1,0:T(8,128)(2,1)} %get-tuple-element.16), channel_id=1, source_target_pairs={{0,4},{4,8},{8,12},{12,16},{16,20},{20,24},{24,28},{28,32},{32,36}... | collective-permute-start | bytes 196616 | tf_op jit(solution)/shard_map/ppermute | solution.py:176
  3.4 0.9 convert_element_type.27
  4.4 119.2 %all-gather.1 = f16[2048,1792]{1,0:T(8,128)(2,1)S(1)} all-gather(f16[32,1792]{1,0:T(8,128)(2,1)S(1)} %convert_element_type.27), channel_id=1, replica_groups=mesh['grp'=2,'sp'=64,'tp'=4] {'sp'}, dimensions={0}, use_global_device_ids=true | all-gather | bytes 7454720 | tf_op jit(solution)/shard_map/all_gather | solution.py:177
  123.6 2.4 %multiply_convert_fusion.2 = (bf16[2048,384]{1,0:T(8,128)(2,1)}, bf16[2048,384]{1,0:T(8,128)(2,1)}) fusion(f16[2048,1792]{1,0:T(8,128)(2,1)S(1)} %all-gather.1), kind=kLoop, calls=%fused_computation.2 | loop fusion | flops 4718592 | bytes 6291456 | tf_op jit(solution)/shard_map/convert_element_type | solution.py:182
  126.0 0.0 copy-start.8
  126.0 2.7 %multiply_convert_fusion = (bf16[2048,512]{1,0:T(8,128)(2,1)}, bf16[2048,512]{1,0:T(8,128)(2,1)}) fusion(f16[2048,1792]{1,0:T(8,128)(2,1)S(1)} %all-gather.1, f32[]{:T(128)} %constant.2.clone.1), kind=kLoop, calls=%fused_computation | loop fusion | flops 6291456 | bytes 8388612 | tf_op jit(solution)/shard_map/convert_element_type | solution.py:182
  128.8 0.0 copy-done.8
  128.8 0.0 collective-permute-done.halo
  128.8 0.0 copy-done
  128.8 0.0 copy-done.5
  128.8 0.0 copy-start.2
  128.8 1.4 copy-done.2
  130.2 1.8 %first.1 = bf16[4,528,128]{2,1,0:T(8,128)(2,1)S(1)} custom-call(s32[1]{0:T(128)} %bitcast.tp_index, bf16[512,2048]{1,0:T(8,128)(2,1)S(1)} %copy-done, bf16[16,2048]{1,0:T(8,128)(2,1)S(1)} %collective-permute-done.halo, bf16[2048,384]{1,0:T(8,128)(2,1)S(1)} %copy-done.2, f32[2,3,512]{2,1,0:T(4,128)S(1)} %copy.10.taps, f32[2,2048]{1,0:T(2,128)S(1)} %copy-done.5), custom_call_target="tpu_custom_call" | custom-call | flops 805306368 | bytes 4194304 | tf_op jit(solution)/shard_map/first/pallas_call | solution.py:189
  132.0 14.6 %all_to_all.10.arrived = bf16[4,528,128]{2,1,0:T(8,128)(2,1)S(1)} all-to-all(bf16[4,528,128]{2,1,0:T(8,128)(2,1)S(1)} %first.1), channel_id=1, replica_groups=mesh['grp'=2,'sp'=64,'tp'=4] {'tp'}, dimensions={0} | all-to-all | bytes 1081344 | tf_op jit(solution)/shard_map/all_to_all | solution.py:202
  146.6 0.0 copy-done.6
  146.6 0.0 copy-done.7
  146.6 0.0 copy-done.3
  146.6 0.0 copy-done.4
  146.6 0.0 copy-start.1
  146.6 4.5 %middle.1 = (bf16[512,128]{1,0:T(8,128)(2,1)S(1)}, f32[128,2048]{1,0:T(8,128)S(1)}) custom-call(s32[1]{0:T(128)} %bitcast.tp_index, bf16[4,528,128]{2,1,0:T(8,128)(2,1)S(1)} %all_to_all.10.arrived, bf16[2048,512]{1,0:T(8,128)(2,1)S(1)} %copy-done.3, bf16[512,2048]{1,0:T(8,128)(2,1)S(1)} %copy-done, bf16[16,2048]{1,0:T(8,128)(2,1)S(1)} %collective-permute-done.halo, ...), custom_call_target="tpu_custom_call" | custom-call | flops 1879048192 | bytes 4194304 | tf_op jit(solution)/shard_map/middle/pallas_call | solution.py:203
  151.1 8.4 %all_to_all.11.arrived = bf16[4,128,128]{2,1,0:T(8,128)(2,1)S(1)} all-to-all(bf16[4,128,128]{2,1,0:T(8,128)(2,1)S(1)} %bitcast.3), channel_id=1, replica_groups=mesh['grp'=2,'sp'=64,'tp'=4] {'tp'}, dimensions={0} | all-to-all | bytes 262144 | tf_op jit(solution)/shard_map/all_to_all | solution.py:220
  159.5 0.0 copy-done.1
  159.5 1.9 %last.1 = bf16[128,2048]{1,0:T(8,128)(2,1)} custom-call(bf16[4,128,128]{2,1,0:T(8,128)(2,1)S(1)} %all_to_all.11.arrived, bf16[2048,512]{1,0:T(8,128)(2,1)S(1)} %copy-done.1, f32[128,2048]{1,0:T(8,128)S(1)} %get-tuple-element.26.residual, f32[2,512]{1,0:T(2,128)S(1)} %copy-done.7, f32[2,2048]{1,0:T(2,128)S(1)} %copy-done.6), custom_call_target="tpu_custom_call" | custom-call | flops 268435456 | bytes 4194304 | tf_op jit(solution)/shard_map/last/pallas_call | solution.py:223
  (7 shorter events, 0.0 us)
Async XLA Ops:
  1.6 127.2 %collective-permute-start = (bf16[16,2048]{1,0:T(8,128)(2,1)}, bf16[16,2048]{1,0:T(8,128)(2,1)S(1)}, u32[]{:S(2)}, u32[]{:S(2)}) collective-permute-start(bf16[16,2048]{1,0:T(8,128)(2,1)} %get-tuple-element.16), channel_id=1, source_target_pairs={{0,4},{4,8},{8,12},{12,16},{16,20},{20,24},{24,28},{28,32},{32,36}... | collective-permute-start | bytes 196616 | tf_op jit(solution)/shard_map/ppermute | solution.py:176
  126.0 2.7 %copy-start.8 = (f32[2,3,512]{2,0,1:T(2,128)S(1)}, f32[2,3,512]{2,0,1:T(2,128)}, u32[]{:S(2)}) copy-start(f32[2,3,512]{2,0,1:T(2,128)} %param.14) | copy-start | bytes 36868
  126.0 2.8 %copy-start = (bf16[512,2048]{1,0:T(8,128)(2,1)S(1)}, bf16[512,2048]{1,0:T(8,128)(2,1)}, u32[]{:S(2)}) copy-start(bf16[512,2048]{1,0:T(8,128)(2,1)} %tokens.3) | copy-start | bytes 6291460
  126.0 2.8 %copy-start.5 = (f32[2,2048]{1,0:T(2,128)S(1)}, f32[2,2048]{1,0:T(2,128)}, u32[]{:S(2)}) copy-start(f32[2,2048]{1,0:T(2,128)} %pre_gain.3) | copy-start | bytes 49156
  128.8 17.8 %copy-start.6 = (f32[2,2048]{1,0:T(2,128)S(1)}, f32[2,2048]{1,0:T(2,128)}, u32[]{:S(2)}) copy-start(f32[2,2048]{1,0:T(2,128)} %post_gain.3) | copy-start | bytes 49156
  128.8 17.8 %copy-start.7 = (f32[2,512]{1,0:T(2,128)S(1)}, f32[2,512]{1,0:T(2,128)}, u32[]{:S(2)}) copy-start(f32[2,512]{1,0:T(2,128)} %mix_gain.3) | copy-start | bytes 12292
  128.8 1.4 copy-start.2
  130.2 16.4 %copy-start.3 = (bf16[2048,512]{1,0:T(8,128)(2,1)S(1)}, bf16[2048,512]{1,0:T(8,128)(2,1)}, u32[]{:S(2)}) copy-start(bf16[2048,512]{1,0:T(8,128)(2,1)} %get-tuple-element.22.out_turned) | copy-start | bytes 6291460
  130.2 16.4 %copy-start.4 = (bf16[2048,384]{1,0:T(8,128)(2,1)S(1)}, bf16[2048,384]{1,0:T(8,128)(2,1)}, u32[]{:S(2)}) copy-start(bf16[2048,384]{1,0:T(8,128)(2,1)} %get-tuple-element.23.gates) | copy-start | bytes 4718596
  146.6 12.9 %copy-start.1 = (bf16[2048,512]{1,0:T(8,128)(2,1)S(1)}, bf16[2048,512]{1,0:T(8,128)(2,1)}, u32[]{:S(2)}) copy-start(bf16[2048,512]{1,0:T(8,128)(2,1)} %get-tuple-element.25.out_turned) | copy-start | bytes 6291460

commit v3 on v2

v3 whole, which is shorter than its diff:
```python
import functools

import jax
import jax.numpy as jnp
from jax import lax
from jax.experimental import pallas as pl
from jax.experimental.pallas import tpu as pltpu
from jax.sharding import PartitionSpec as P

EPS = 1e-06
GATE_SCALE = 2.0**18
OUT_SCALE = 2.0**17
HALO = 16
PAD = 8
BLOCK = 128
VMEM_LIMIT = 16 * 1024 * 1024


def scale_of(values, count):
    return lax.rsqrt(jnp.sum(values * values, axis=-1, keepdims=True) * (1.0 / count) + EPS)


def pack_kernel(gate_in, gate_conv, value_in, out_turned, tail, packed, tail_out):
    layers, _, channels = gate_in.shape
    whole = out_turned.shape[2]
    start = 0
    for layer in range(layers):
        for w in (gate_in, gate_conv, value_in):
            scaled = w[layer].astype(jnp.float32) * GATE_SCALE
            packed[:, start : start + channels] = scaled.astype(jnp.bfloat16)
            start += channels
        scaled = out_turned[layer].astype(jnp.float32) * OUT_SCALE
        packed[:, start : start + whole] = scaled.astype(jnp.bfloat16)
        start += whole
    tail_out[...] = tail[...]


def pack(tokens, gate_in, gate_conv, value_in, out_turned):
    rows = gate_in.shape[1]
    columns = gate_in.shape[0] * (3 * gate_in.shape[2] + out_turned.shape[2])
    count, width = tokens.shape
    return pl.pallas_call(
        pack_kernel,
        grid=(1,),
        in_specs=[
            pl.BlockSpec(gate_in.shape, lambda i: (0, 0, 0)),
            pl.BlockSpec(gate_in.shape, lambda i: (0, 0, 0)),
            pl.BlockSpec(gate_in.shape, lambda i: (0, 0, 0)),
            pl.BlockSpec(out_turned.shape, lambda i: (0, 0, 0)),
            pl.BlockSpec((HALO, width), lambda i: (count // HALO - 1, 0)),
        ],
        out_specs=[
            pl.BlockSpec((rows, columns), lambda i: (0, 0)),
            pl.BlockSpec((HALO, width), lambda i: (0, 0)),
        ],
        out_shape=[
            jax.ShapeDtypeStruct((rows, columns), jnp.bfloat16),
            jax.ShapeDtypeStruct((HALO, width), jnp.bfloat16),
        ],
        name="pack",
    )(gate_in, gate_conv, value_in, out_turned, tokens)


def in_blocks(rows):
    return [(0, HALO)] + [(HALO + start, BLOCK) for start in range(0, rows, BLOCK)]


def normed_kernel(tokens, halo, pre_gain, normed):
    row_count, width = tokens.shape
    for first, count in in_blocks(row_count):
        rows = halo[...] if first == 0 else tokens[first - HALO : first - HALO + count, :]
        stream = rows.astype(jnp.float32)
        scale = scale_of(stream, width)
        normed[first : first + count, :] = (stream * scale * pre_gain[0:1, :]).astype(jnp.bfloat16)


def mix_kernel(layer, spread, tp_index, mixers, taps, raw, gated_rows):
    rows = mixers.shape[0]
    tap_count = taps.shape[1]
    channels = mixers.shape[1] // 3
    mine = pl.ds(pl.multiple_of(tp_index[0] * channels, channels), channels)
    gated = mixers[:, channels : 2 * channels].astype(jnp.float32)
    gated = gated * mixers[:, 2 * channels :].astype(jnp.float32)
    gated_rows[0:PAD, :] = jnp.zeros((PAD, channels), jnp.float32)
    gated_rows[PAD:, :] = gated.astype(jnp.bfloat16).astype(jnp.float32)
    filtered = None
    for tap in range(tap_count):
        at = PAD - (tap_count - 1) + tap
        term = taps[layer, tap : tap + 1, mine] * gated_rows[at : at + rows, :]
        filtered = term if filtered is None else filtered + term
    values = (mixers[:, :channels].astype(jnp.float32) * filtered).astype(jnp.bfloat16)
    if spread:
        for t in range(raw.shape[0]):
            raw[t] = values
    else:
        raw[...] = values[HALO:, :]


def mixed_kernel(layer, arrived, mix_gain, mixed):
    parts = [arrived[t].astype(jnp.float32) for t in range(arrived.shape[0])]
    values = jnp.concatenate(parts, axis=1)
    scale = scale_of(values, values.shape[1])
    mixed[...] = (values * scale * mix_gain[layer : layer + 1, :]).astype(jnp.bfloat16)


def added(stream, branch, post_gain, layer):
    branch = branch.astype(jnp.float32)
    return stream + branch * scale_of(branch, branch.shape[1]) * post_gain[layer : layer + 1, :]


def middle_kernel(tp_index, branch, tokens, halo, post_gain, pre_gain, normed, residual):
    row_count, width = tokens.shape
    for first, count in in_blocks(row_count):
        rows = halo[...] if first == 0 else tokens[first - HALO : first - HALO + count, :]
        stream = added(rows.astype(jnp.float32), branch[first : first + count, :], post_gain, 0)
        if first > 0:

            @pl.when(tp_index[0] == (first - HALO) // BLOCK)
            def _():
                residual[...] = stream

        scale = scale_of(stream, width)
        normed[first : first + count, :] = (stream * scale * pre_gain[1:2, :]).astype(jnp.bfloat16)


def last_kernel(branch, residual, post_gain, result):
    result[...] = added(residual[...], branch[...], post_gain, 1).astype(jnp.bfloat16)


def per_device(
    tokens, gate_in, gate_conv, value_in, out_weight, conv_taps, pre_gain, mix_gain, post_gain
):
    channels = gate_in.shape[2]
    whole = out_weight.shape[1]
    row_count, width = tokens.shape
    all_rows = HALO + row_count
    tp_size = lax.axis_size("tp")
    sp_size = lax.axis_size("sp")
    tp_index = lax.axis_index("tp").reshape(1)
    share = row_count // tp_size
    params = pltpu.CompilerParams(vmem_limit_bytes=VMEM_LIMIT)
    smem = pl.BlockSpec(memory_space=pltpu.SMEM)
    vmem = pl.BlockSpec(memory_space=pltpu.VMEM)

    def call(kernel, name, in_specs, shapes, *operands, scratch=()):
        return pl.pallas_call(
            kernel,
            in_specs=in_specs,
            out_specs=[vmem] * len(shapes),
            out_shape=[jax.ShapeDtypeStruct(shape, dtype) for shape, dtype in shapes],
            scratch_shapes=list(scratch),
            compiler_params=params,
            cost_estimate=pl.CostEstimate(flops=1 << 26, bytes_accessed=4 << 20, transcendentals=0),
            name=name,
        )(*operands)

    packed, tail = pack(tokens, gate_in, gate_conv, value_in, jnp.swapaxes(out_weight, 1, 2))
    halo = lax.ppermute(tail, "sp", [(i, i + 1) for i in range(sp_size - 1)])
    gathered = lax.all_gather(packed.astype(jnp.float16), "sp", axis=0, tiled=True)
    stride = 3 * channels + whole

    def gates(layer):
        part = gathered[:, layer * stride : layer * stride + 3 * channels]
        return (part.astype(jnp.float32) * (1.0 / GATE_SCALE)).astype(jnp.bfloat16)

    def out_turned(layer):
        part = gathered[:, layer * stride + 3 * channels : (layer + 1) * stride]
        return (part.astype(jnp.float32) * (1.0 / OUT_SCALE)).astype(jnp.bfloat16)

    def mixers_of(normed, layer):
        return jnp.dot(normed, gates(layer), preferred_element_type=jnp.float32).astype(jnp.bfloat16)

    def branch_of(mixed, layer):
        product = lax.dot_general(
            mixed, out_turned(layer), (((1,), (1,)), ((), ())), preferred_element_type=jnp.float32
        )
        return product.astype(jnp.bfloat16)

    gated_rows = pltpu.VMEM((PAD + all_rows, channels), jnp.float32)
    bf16, f32 = jnp.bfloat16, jnp.float32
    (normed,) = call(normed_kernel, "normed", [vmem] * 3, [((all_rows, width), bf16)], tokens, halo, pre_gain)
    (raw,) = call(
        functools.partial(mix_kernel, 0, True), "mix0", [smem, vmem, vmem],
        [((tp_size, all_rows, channels), bf16)], tp_index, mixers_of(normed, 0), conv_taps, scratch=(gated_rows,),
    )
    arrived = lax.all_to_all(raw, "tp", split_axis=0, concat_axis=0, tiled=True)
    (mixed,) = call(
        functools.partial(mixed_kernel, 0), "mixed0", [vmem] * 2, [((all_rows, whole), bf16)], arrived, mix_gain
    )
    normed, residual = call(
        middle_kernel, "middle", [smem] + [vmem] * 5, [((all_rows, width), bf16), ((share, width), f32)],
        tp_index, branch_of(mixed, 0), tokens, halo, post_gain, pre_gain,
    )
    (raw,) = call(
        functools.partial(mix_kernel, 1, False), "mix1", [smem, vmem, vmem],
        [((row_count, channels), bf16)], tp_index, mixers_of(normed, 1), conv_taps, scratch=(gated_rows,),
    )
    arrived = lax.all_to_all(
        raw.reshape(tp_size, share, channels), "tp", split_axis=0, concat_axis=0, tiled=True
    )
    (mixed,) = call(
        functools.partial(mixed_kernel, 1), "mixed1", [vmem] * 2, [((share, whole), bf16)], arrived, mix_gain
    )
    (result,) = call(
        last_kernel, "last", [vmem] * 3, [((share, width), bf16)], branch_of(mixed, 1), residual, post_gain
    )
    return result


def solution(mesh):
    placed = (
        P(("grp", "sp"), None),
        P(None, "sp", "tp"),
        P(None, "sp", "tp"),
        P(None, "sp", "tp"),
        P(None, None, "sp"),
        P(),
        P(),
        P(),
        P(),
    )
    return jax.shard_map(
        per_device,
        mesh=mesh,
        in_specs=placed,
        out_specs=P(("grp", "sp", "tp"), None),
        check_vma=False,
    )
```

time: 162 us -> 161 us (level)
  matrix products: 0 us -> 6.6 us
  other arithmetic: 6.07 us -> 0.92 us
  Pallas kernels: 9.74 us -> 6.48 us
  blocking collectives: 142 us -> 144 us
    dot_general x0 -> x4, matrix products: none -> 6.6 us  [the longest x2 4.42 us: mixers_of(): jnp.dot(normed, gates(layer), preferred_element_type=jnp.float32)]
    convert_element_type x2 -> x0, other arithmetic: 5.15 us -> none  [received(): return part.astype(jnp.bfloat16)]
    pallas_call x3 -> x7, Pallas kernels: 8.14 us -> 4.88 us  [call(): pl.pallas_call(kernel, in_specs=in_specs, out_specs=[vmem] * len(shapes),...]
    all_gather x1, blocking collectives: 119 us -> 121 us  [per_device(): lax.all_gather(packed.astype(jnp.float16), 'sp', axis=0, tiled=True)]
  transfers between devices with their start and end apart: 1 -> 1, of which waited for: 0 -> 0; matrix products, arithmetic and copies ran while one was open for 4% -> 1% of each run, Pallas kernels for 0% -> 0%
where the time goes in v3:
time: 161 us; the launch traced here: 160 us
  blocking collectives  144 us (89%)
  matrix products  6.6 us (4%)
  Pallas kernels  6.48 us (4%)
  starting transfers between devices  1.83 us (1%)
    all_gather x1, blocking collectives, per_device(): lax.all_gather(packed.astype(jnp.float16), 'sp', axis=0, tiled=True)  121 us
    all_to_all x1, blocking collectives, per_device(): arrived = lax.all_to_all(raw, 'tp', split_axis=0, concat_axis=0, tiled=True)  14.6 us
    all_to_all x1, blocking collectives, per_device(): lax.all_to_all(raw.reshape(tp_size, share, channels), 'tp', split_axis=0,...  8.39 us
    pallas_call x7, Pallas kernels, call(): pl.pallas_call(kernel, in_specs=in_specs, out_specs=[vmem] * len(shapes),...  4.88 us
    dot_general x2, matrix products, mixers_of(): jnp.dot(normed, gates(layer), preferred_element_type=jnp.float32)  4.42 us
  transfers between devices with their start and end apart: 1, of which 0 were waited for; matrix products, arithmetic and copies ran while one was open for 1% of the time, Pallas kernels for 0%

profile of v3, /device:TPU:40, one launch (start us, length us, event | category | flops | bytes accessed | tf_op | source)
XLA Modules:
  0.0 160.4 jit_solution(2173604923750159181)
XLA Ops:
  0.0 1.6 pack.1
  1.6 1.8 %collective-permute-start = (bf16[16,2048]{1,0:T(8,128)(2,1)}, bf16[16,2048]{1,0:T(8,128)(2,1)S(1)}, u32[]{:S(2)}, u32[]{:S(2)}) collective-permute-start(bf16[16,2048]{1,0:T(8,128)(2,1)} %get-tuple-element.9), channel_id=1, source_target_pairs={{0,4},{4,8},{8,12},{12,16},{16,20},{20,24},{24,28},{28,32},{32,36}... | collective-permute-start | bytes 196616 | tf_op jit(solution)/shard_map/ppermute | solution.py:158
  3.4 0.9 convert_element_type.39
  4.4 0.0 copy-start.4
  4.4 0.0 copy-start
  4.4 0.0 copy-start.1
  4.4 121.4 %all-gather.1 = f16[2048,1792]{1,0:T(8,128)(2,1)} all-gather(f16[32,1792]{1,0:T(8,128)(2,1)S(1)} %convert_element_type.39), channel_id=1, replica_groups=mesh['grp'=2,'sp'=64,'tp'=4] {'sp'}, dimensions={0}, use_global_device_ids=true | all-gather | bytes 7454720 | tf_op jit(solution)/shard_map/all_gather | solution.py:159
  125.8 0.0 slice-start
  125.8 0.8 normed.1
  126.7 0.0 copy-start.3
  126.7 0.0 slice-start.1
  126.7 3.1 %fusion.11.mixers = bf16[528,384]{1,0:T(8,128)(2,1)S(1)} fusion(bf16[528,2048]{1,0:T(8,128)(2,1)S(1)} %normed.1, f16[2048,1792]{1,0:T(8,128)(2,1)} %all-gather.1), kind=kOutput, calls=%fused_computation.17 | convolution fusion | flops 833034240 | bytes 4141056 | tf_op jit(solution)/shard_map/dot_general | solution.py:171
  129.8 0.2 mix0.1
  130.1 14.6 %all_to_all.10.arrived = bf16[4,528,128]{2,1,0:T(8,128)(2,1)S(1)} all-to-all(bf16[4,528,128]{2,1,0:T(8,128)(2,1)S(1)} %mix0.1), channel_id=1, replica_groups=mesh['grp'=2,'sp'=64,'tp'=4] {'tp'}, dimensions={0} | all-to-all | bytes 1081344 | tf_op jit(solution)/shard_map/all_to_all | solution.py:186
  144.6 0.3 mixed0.1
  144.9 0.0 copy-start.2
  144.9 1.3 convolution_convert_fusion.branch
  146.3 2.1 %middle.1 = (bf16[528,2048]{1,0:T(8,128)(2,1)S(1)}, f32[128,2048]{1,0:T(8,128)S(1)}) custom-call(s32[1]{0:T(128)} %bitcast.tp_index, bf16[528,2048]{1,0:T(8,128)(2,1)S(1)} %convolution_convert_fusion.branch, bf16[512,2048]{1,0:T(8,128)(2,1)S(1)} %copy-done, bf16[16,2048]{1,0:T(8,128)(2,1)S(1)} %collective-permute-done.halo, f32[2,2048]{1,0:T(2,128)S(1)} %copy-done.2, ...), custom_call_target="tpu_custom_call" | custom-call | flops 67108864 | bytes 4194304 | tf_op jit(solution)/shard_map/middle/pallas_call | solution.py:146
  148.3 1.3 fusion.10.mixers
  149.6 0.2 mix1.1
  149.8 8.4 %all_to_all.11.arrived = bf16[4,128,128]{2,1,0:T(8,128)(2,1)S(1)} all-to-all(bf16[4,128,128]{2,1,0:T(8,128)(2,1)S(1)} %bitcast.7), channel_id=1, replica_groups=mesh['grp'=2,'sp'=64,'tp'=4] {'tp'}, dimensions={0} | all-to-all | bytes 262144 | tf_op jit(solution)/shard_map/all_to_all | solution.py:198
  158.2 0.1 mixed1.1
  158.3 0.8 convolution_convert_fusion.1.branch
  159.2 1.2 last.1
  (10 shorter events, 0.0 us)
Async XLA Ops:
  1.6 124.2 %collective-permute-start = (bf16[16,2048]{1,0:T(8,128)(2,1)}, bf16[16,2048]{1,0:T(8,128)(2,1)S(1)}, u32[]{:S(2)}, u32[]{:S(2)}) collective-permute-start(bf16[16,2048]{1,0:T(8,128)(2,1)} %get-tuple-element.9), channel_id=1, source_target_pairs={{0,4},{4,8},{8,12},{12,16},{16,20},{20,24},{24,28},{28,32},{32,36}... | collective-permute-start | bytes 196616 | tf_op jit(solution)/shard_map/ppermute | solution.py:158
  4.4 121.4 %copy-start.4 = (f32[2,3,512]{2,0,1:T(2,128)S(1)}, f32[2,3,512]{2,0,1:T(2,128)}, u32[]{:S(2)}) copy-start(f32[2,3,512]{2,0,1:T(2,128)} %param.14) | copy-start | bytes 36868
  4.4 121.4 %copy-start = (bf16[512,2048]{1,0:T(8,128)(2,1)S(1)}, bf16[512,2048]{1,0:T(8,128)(2,1)}, u32[]{:S(2)}) copy-start(bf16[512,2048]{1,0:T(8,128)(2,1)} %tokens.3) | copy-start | bytes 6291460
  4.4 121.4 %copy-start.1 = (f32[2,2048]{1,0:T(2,128)S(1)}, f32[2,2048]{1,0:T(2,128)}, u32[]{:S(2)}) copy-start(f32[2,2048]{1,0:T(2,128)} %pre_gain.3) | copy-start | bytes 49156
  125.8 19.0 %slice-start = ((s8[7340032]{0:T(1024)(128)(4,1)}), s8[4194304]{0:T(1024)(128)(4,1)S(1)}, s32[]{:S(2)}) async-start(s8[7340032]{0:T(1024)(128)(4,1)} %bitcast.8), calls=%async_computation.2 | async-start | bytes 8388608
  126.7 17.9 %copy-start.3 = (f32[2,512]{1,0:T(2,128)S(1)}, f32[2,512]{1,0:T(2,128)}, u32[]{:S(2)}) copy-start(f32[2,512]{1,0:T(2,128)} %mix_gain.3) | copy-start | bytes 12292
  126.7 18.2 %slice-start.1 = ((s8[7340032]{0:T(1024)(128)(4,1)}), s8[3145728]{0:T(1024)(128)(4,1)S(1)}, s32[]{:S(2)}) async-start(s8[7340032]{0:T(1024)(128)(4,1)} %bitcast.8), calls=%async_computation.3 | async-start | bytes 6291456
  144.9 1.4 copy-start.2

commit v4 on v3

--- a/solution.py
+++ b/solution.py
@@ -20,7 +20,23 @@
     return lax.rsqrt(jnp.sum(values * values, axis=-1, keepdims=True) * (1.0 / count) + EPS)
 
 
-def pack_kernel(gate_in, gate_conv, value_in, out_turned, tail, packed, tail_out):
+def tail_kernel(tail, tail_out):
+    tail_out[...] = tail[...]
+
+
+def tail_of(tokens):
+    count, width = tokens.shape
+    return pl.pallas_call(
+        tail_kernel,
+        grid=(1,),
+        in_specs=[pl.BlockSpec((HALO, width), lambda i: (count // HALO - 1, 0))],
+        out_specs=pl.BlockSpec((HALO, width), lambda i: (0, 0)),
+        out_shape=jax.ShapeDtypeStruct((HALO, width), jnp.bfloat16),
+        name="tail",
+    )(tokens)
+
+
+def pack_kernel(gate_in, gate_conv, value_in, out_turned, packed):
     layers, _, channels = gate_in.shape
     whole = out_turned.shape[2]
     start = 0
@@ -32,13 +48,11 @@
         scaled = out_turned[layer].astype(jnp.float32) * OUT_SCALE
         packed[:, start : start + whole] = scaled.astype(jnp.bfloat16)
         start += whole
-    tail_out[...] = tail[...]
-
-
-def pack(tokens, gate_in, gate_conv, value_in, out_turned):
+
+
+def pack(gate_in, gate_conv, value_in, out_turned):
     rows = gate_in.shape[1]
     columns = gate_in.shape[0] * (3 * gate_in.shape[2] + out_turned.shape[2])
-    count, width = tokens.shape
     return pl.pallas_call(
         pack_kernel,
         grid=(1,),
@@ -47,18 +61,11 @@
             pl.BlockSpec(gate_in.shape, lambda i: (0, 0, 0)),
             pl.BlockSpec(gate_in.shape, lambda i: (0, 0, 0)),
             pl.BlockSpec(out_turned.shape, lambda i: (0, 0, 0)),
-            pl.BlockSpec((HALO, width), lambda i: (count // HALO - 1, 0)),
         ],
-        out_specs=[
-            pl.BlockSpec((rows, columns), lambda i: (0, 0)),
-            pl.BlockSpec((HALO, width), lambda i: (0, 0)),
-        ],
-        out_shape=[
-            jax.ShapeDtypeStruct((rows, columns), jnp.bfloat16),
-            jax.ShapeDtypeStruct((HALO, width), jnp.bfloat16),
-        ],
+        out_specs=pl.BlockSpec((rows, columns), lambda i: (0, 0)),
+        out_shape=jax.ShapeDtypeStruct((rows, columns), jnp.bfloat16),
         name="pack",
-    )(gate_in, gate_conv, value_in, out_turned, tokens)
+    )(gate_in, gate_conv, value_in, out_turned)
 
 
 def in_blocks(rows):
@@ -154,9 +161,12 @@
             name=name,
         )(*operands)
 
-    packed, tail = pack(tokens, gate_in, gate_conv, value_in, jnp.swapaxes(out_weight, 1, 2))
-    halo = lax.ppermute(tail, "sp", [(i, i + 1) for i in range(sp_size - 1)])
-    gathered = lax.all_gather(packed.astype(jnp.float16), "sp", axis=0, tiled=True)
+    packed = pack(gate_in, gate_conv, value_in, jnp.swapaxes(out_weight, 1, 2))
+    halo = lax.ppermute(tail_of(tokens), "sp", [(i, i + 1) for i in range(sp_size - 1)])
+    bf16, f32 = jnp.bfloat16, jnp.float32
+    (normed,) = call(normed_kernel, "normed", [vmem] * 3, [((all_rows, width), bf16)], tokens, halo, pre_gain)
+    sent, normed = lax.optimization_barrier((packed.astype(jnp.float16), normed))
+    gathered = lax.all_gather(sent, "sp", axis=0, tiled=True)
     stride = 3 * channels + whole
 
     def gates(layer):
@@ -177,8 +187,6 @@
         return product.astype(jnp.bfloat16)
 
     gated_rows = pltpu.VMEM((PAD + all_rows, channels), jnp.float32)
-    bf16, f32 = jnp.bfloat16, jnp.float32
-    (normed,) = call(normed_kernel, "normed", [vmem] * 3, [((all_rows, width), bf16)], tokens, halo, pre_gain)
     (raw,) = call(
         functools.partial(mix_kernel, 0, True), "mix0", [smem, vmem, vmem],
         [((tp_size, all_rows, channels), bf16)], tp_index, mixers_of(normed, 0), conv_taps, scratch=(gated_rows,),

time: 161 us -> 160 us (level)
  matrix products: 6.6 us -> 4.8 us
    dot_general x2, matrix products: 4.42 us -> 2.61 us  [mixers_of(): jnp.dot(normed, gates(layer), preferred_element_type=jnp.float32)]
    pallas_call x0 -> x1, Pallas kernels: none -> 1.63 us  [tail_of(): pl.pallas_call(tail_kernel, grid=(1,), in_specs=[pl.BlockSpec((HALO, widt...]
  transfers between devices with their start and end apart: 1 -> 1, of which waited for: 0 -> 0; matrix products, arithmetic and copies ran while one was open for 1% -> 1% of each run, Pallas kernels for 0% -> 1%
where the time goes in v4:
time: 160 us
  blocking collectives  144 us (90%)
  Pallas kernels  8.07 us (5%)
  matrix products  4.8 us (3%)
  starting transfers between devices  1.83 us (1%)
    all_gather x1, blocking collectives, per_device(): gathered = lax.all_gather(sent, 'sp', axis=0, tiled=True)  121 us
    all_to_all x1, blocking collectives, per_device(): arrived = lax.all_to_all(raw, 'tp', split_axis=0, concat_axis=0, tiled=True)  14.6 us
    all_to_all x1, blocking collectives, per_device(): lax.all_to_all(raw.reshape(tp_size, share, channels), 'tp', split_axis=0,...  8.39 us
    pallas_call x7, Pallas kernels, call(): pl.pallas_call(kernel, in_specs=in_specs, out_specs=[vmem] * len(shapes),...  4.88 us
  transfers between devices with their start and end apart: 1, of which 0 were waited for; matrix products, arithmetic and copies ran while one was open for 1% of the time, Pallas kernels for 1%

profile of v4, /device:TPU:40, one launch (start us, length us, event | category | flops | bytes accessed | tf_op | source)
XLA Modules:
  0.0 160.1 jit_solution(16939303657184637045)
XLA Ops:
  0.0 1.6 %tail.2 = bf16[16,2048]{1,0:T(8,128)(2,1)} custom-call(bf16[512,2048]{1,0:T(8,128)(2,1)} %tokens.3), custom_call_target="tpu_custom_call" | custom-call | tf_op jit(solution)/shard_map/tail/pallas_call | solution.py:29
  1.6 1.8 %collective-permute-start = (bf16[16,2048]{1,0:T(8,128)(2,1)}, bf16[16,2048]{1,0:T(8,128)(2,1)S(1)}, u32[]{:S(2)}, u32[]{:S(2)}) collective-permute-start(bf16[16,2048]{1,0:T(8,128)(2,1)} %tail.2), channel_id=1, source_target_pairs={{0,4},{4,8},{8,12},{12,16},{16,20},{20,24},{24,28},{28,32},{32,36}... | collective-permute-start | bytes 196616 | tf_op jit(solution)/shard_map/ppermute | solution.py:165
  3.5 0.0 copy-done.4
  3.5 1.6 pack.1
  5.1 0.9 convert_element_type.39
  6.0 0.0 collective-permute-done.halo
  6.0 0.0 copy-done
  6.0 0.0 copy-done.1
  6.0 0.8 normed.1
  6.9 121.4 %all-gather.1 = f16[2048,1792]{1,0:T(8,128)(2,1)S(1)} all-gather(f16[32,1792]{1,0:T(8,128)(2,1)S(1)} %convert_element_type.39), channel_id=1, replica_groups=mesh['grp'=2,'sp'=64,'tp'=4] {'sp'}, dimensions={0}, use_global_device_ids=true | all-gather | bytes 7454720 | tf_op jit(solution)/shard_map/all_gather | solution.py:169
  128.3 1.3 fusion.11.mixers
  129.6 0.2 mix0.1
  129.8 14.6 %all_to_all.10.arrived = bf16[4,528,128]{2,1,0:T(8,128)(2,1)S(1)} all-to-all(bf16[4,528,128]{2,1,0:T(8,128)(2,1)S(1)} %mix0.1), channel_id=1, replica_groups=mesh['grp'=2,'sp'=64,'tp'=4] {'tp'}, dimensions={0} | all-to-all | bytes 1081344 | tf_op jit(solution)/shard_map/all_to_all | solution.py:194
  144.4 0.3 mixed0.1
  144.6 0.0 copy-start.2
  144.6 1.3 convolution_convert_fusion.branch
  146.0 0.0 copy-done.2
  146.0 2.1 %middle.1 = (bf16[528,2048]{1,0:T(8,128)(2,1)S(1)}, f32[128,2048]{1,0:T(8,128)S(1)}) custom-call(s32[1]{0:T(128)} %bitcast.tp_index, bf16[528,2048]{1,0:T(8,128)(2,1)S(1)} %convolution_convert_fusion.branch, bf16[512,2048]{1,0:T(8,128)(2,1)S(1)} %copy-done, bf16[16,2048]{1,0:T(8,128)(2,1)S(1)} %collective-permute-done.halo, f32[2,2048]{1,0:T(2,128)S(1)} %copy-done.2, ...), custom_call_target="tpu_custom_call" | custom-call | flops 67108864 | bytes 4194304 | tf_op jit(solution)/shard_map/middle/pallas_call | solution.py:153
  148.1 1.3 fusion.10.mixers
  149.4 0.2 mix1.1
  149.5 8.4 %all_to_all.11.arrived = bf16[4,128,128]{2,1,0:T(8,128)(2,1)S(1)} all-to-all(bf16[4,128,128]{2,1,0:T(8,128)(2,1)S(1)} %bitcast.7), channel_id=1, replica_groups=mesh['grp'=2,'sp'=64,'tp'=4] {'tp'}, dimensions={0} | all-to-all | bytes 262144 | tf_op jit(solution)/shard_map/all_to_all | solution.py:206
  157.9 0.1 mixed1.1
  158.1 0.8 convolution_convert_fusion.1.branch
  158.9 1.2 last.1
  (6 shorter events, 0.0 us)
Async XLA Ops:
  0.0 6.0 %copy-start = (bf16[512,2048]{1,0:T(8,128)(2,1)S(1)}, bf16[512,2048]{1,0:T(8,128)(2,1)}, u32[]{:S(2)}) copy-start(bf16[512,2048]{1,0:T(8,128)(2,1)} %tokens.3) | copy-start | bytes 6291460
  0.0 3.5 %copy-start.4 = (f32[2,3,512]{2,0,1:T(2,128)S(1)}, f32[2,3,512]{2,0,1:T(2,128)}, u32[]{:S(2)}) copy-start(f32[2,3,512]{2,0,1:T(2,128)} %param.14) | copy-start | bytes 36868
  0.0 6.0 %copy-start.1 = (f32[2,2048]{1,0:T(2,128)S(1)}, f32[2,2048]{1,0:T(2,128)}, u32[]{:S(2)}) copy-start(f32[2,2048]{1,0:T(2,128)} %pre_gain.3) | copy-start | bytes 49156
  1.6 4.4 %collective-permute-start = (bf16[16,2048]{1,0:T(8,128)(2,1)}, bf16[16,2048]{1,0:T(8,128)(2,1)S(1)}, u32[]{:S(2)}, u32[]{:S(2)}) collective-permute-start(bf16[16,2048]{1,0:T(8,128)(2,1)} %tail.2), channel_id=1, source_target_pairs={{0,4},{4,8},{8,12},{12,16},{16,20},{20,24},{24,28},{28,32},{32,36}... | collective-permute-start | bytes 196616 | tf_op jit(solution)/shard_map/ppermute | solution.py:165
  128.3 16.1 %copy-start.3 = (f32[2,512]{1,0:T(2,128)S(1)}, f32[2,512]{1,0:T(2,128)}, u32[]{:S(2)}) copy-start(f32[2,512]{1,0:T(2,128)} %mix_gain.3) | copy-start | bytes 12292
  144.6 1.4 copy-start.2

commit v5 on v4

--- a/solution.py
+++ b/solution.py
@@ -10,7 +10,7 @@
 EPS = 1e-06
 GATE_SCALE = 2.0**18
 OUT_SCALE = 2.0**17
-HALO = 16
+HALO = 8
 PAD = 8
 BLOCK = 128
 VMEM_LIMIT = 16 * 1024 * 1024

time: 160 us -> 159 us (level)
  no operation moved by 1% of the time
where the time goes in v5:
time: 159 us
  blocking collectives  143 us (90%)
  Pallas kernels  7.89 us (5%)
  matrix products  4.77 us (3%)
  starting transfers between devices  1.83 us (1%)
    all_gather x1, blocking collectives, per_device(): gathered = lax.all_gather(sent, 'sp', axis=0, tiled=True)  121 us
    all_to_all x1, blocking collectives, per_device(): arrived = lax.all_to_all(raw, 'tp', split_axis=0, concat_axis=0, tiled=True)  14.5 us
    all_to_all x1, blocking collectives, per_device(): lax.all_to_all(raw.reshape(tp_size, share, channels), 'tp', split_axis=0,...  8.39 us
    pallas_call x7, Pallas kernels, call(): pl.pallas_call(kernel, in_specs=in_specs, out_specs=[vmem] * len(shapes),...  4.79 us
  transfers between devices with their start and end apart: 1, of which 0 were waited for; matrix products, arithmetic and copies ran while one was open for 1% of the time, Pallas kernels for 1%

profile of v5, /device:TPU:40, one launch (start us, length us, event | category | flops | bytes accessed | tf_op | source)
XLA Modules:
  0.0 159.0 jit_solution(10140088873740613151)
XLA Ops:
  0.0 1.5 tail.2
  1.5 1.8 %collective-permute-start = (bf16[8,2048]{1,0:T(8,128)(2,1)}, bf16[8,2048]{1,0:T(8,128)(2,1)S(1)}, u32[]{:S(2)}, u32[]{:S(2)}) collective-permute-start(bf16[8,2048]{1,0:T(8,128)(2,1)} %tail.2), channel_id=1, source_target_pairs={{0,4},{4,8},{8,12},{12,16},{16,20},{20,24},{24,28},{28,32},{32,36}... | collective-permute-start | bytes 98312 | tf_op jit(solution)/shard_map/ppermute | solution.py:165
  3.4 0.0 copy-done.4
  3.4 1.6 pack.1
  5.0 0.9 convert_element_type.39
  5.9 0.0 collective-permute-done.halo
  5.9 0.0 copy-done
  5.9 0.0 copy-done.1
  5.9 0.8 normed.1
  6.8 120.5 %all-gather.1 = f16[2048,1792]{1,0:T(8,128)(2,1)S(1)} all-gather(f16[32,1792]{1,0:T(8,128)(2,1)S(1)} %convert_element_type.39), channel_id=1, replica_groups=mesh['grp'=2,'sp'=64,'tp'=4] {'sp'}, dimensions={0}, use_global_device_ids=true | all-gather | bytes 7454720 | tf_op jit(solution)/shard_map/all_gather | solution.py:169
  127.3 1.3 fusion.11.mixers
  128.6 0.2 mix0.1
  128.8 14.5 %all_to_all.10.arrived = bf16[4,520,128]{2,1,0:T(8,128)(2,1)S(1)} all-to-all(bf16[4,520,128]{2,1,0:T(8,128)(2,1)S(1)} %mix0.1), channel_id=1, replica_groups=mesh['grp'=2,'sp'=64,'tp'=4] {'tp'}, dimensions={0} | all-to-all | bytes 1064960 | tf_op jit(solution)/shard_map/all_to_all | solution.py:194
  143.3 0.0 copy-done.3
  143.3 0.2 mixed0.1
  143.5 0.0 copy-start.2
  143.5 1.3 convolution_convert_fusion.branch
  144.9 2.0 %middle.1 = (bf16[520,2048]{1,0:T(8,128)(2,1)S(1)}, f32[128,2048]{1,0:T(8,128)S(1)}) custom-call(s32[1]{0:T(128)} %bitcast.tp_index, bf16[520,2048]{1,0:T(8,128)(2,1)S(1)} %convolution_convert_fusion.branch, bf16[512,2048]{1,0:T(8,128)(2,1)S(1)} %copy-done, bf16[8,2048]{1,0:T(8,128)(2,1)S(1)} %collective-permute-done.halo, f32[2,2048]{1,0:T(2,128)S(1)} %copy-done.2, ...), custom_call_target="tpu_custom_call" | custom-call | flops 67108864 | bytes 4194304 | tf_op jit(solution)/shard_map/middle/pallas_call | solution.py:153
  146.9 1.3 fusion.10.mixers
  148.2 0.2 mix1.1
  148.4 8.4 %all_to_all.11.arrived = bf16[4,128,128]{2,1,0:T(8,128)(2,1)S(1)} all-to-all(bf16[4,128,128]{2,1,0:T(8,128)(2,1)S(1)} %bitcast.7), channel_id=1, replica_groups=mesh['grp'=2,'sp'=64,'tp'=4] {'tp'}, dimensions={0} | all-to-all | bytes 262144 | tf_op jit(solution)/shard_map/all_to_all | solution.py:206
  156.8 0.1 mixed1.1
  156.9 0.8 convolution_convert_fusion.1.branch
  157.8 1.2 last.1
  (6 shorter events, 0.0 us)
Async XLA Ops:
  0.0 5.9 %copy-start = (bf16[512,2048]{1,0:T(8,128)(2,1)S(1)}, bf16[512,2048]{1,0:T(8,128)(2,1)}, u32[]{:S(2)}) copy-start(bf16[512,2048]{1,0:T(8,128)(2,1)} %tokens.3) | copy-start | bytes 6291460
  0.0 3.4 %copy-start.4 = (f32[2,3,512]{2,0,1:T(2,128)S(1)}, f32[2,3,512]{2,0,1:T(2,128)}, u32[]{:S(2)}) copy-start(f32[2,3,512]{2,0,1:T(2,128)} %param.14) | copy-start | bytes 36868
  0.0 5.9 %copy-start.1 = (f32[2,2048]{1,0:T(2,128)S(1)}, f32[2,2048]{1,0:T(2,128)}, u32[]{:S(2)}) copy-start(f32[2,2048]{1,0:T(2,128)} %pre_gain.3) | copy-start | bytes 49156
  1.5 4.4 %collective-permute-start = (bf16[8,2048]{1,0:T(8,128)(2,1)}, bf16[8,2048]{1,0:T(8,128)(2,1)S(1)}, u32[]{:S(2)}, u32[]{:S(2)}) collective-permute-start(bf16[8,2048]{1,0:T(8,128)(2,1)} %tail.2), channel_id=1, source_target_pairs={{0,4},{4,8},{8,12},{12,16},{16,20},{20,24},{24,28},{28,32},{32,36}... | collective-permute-start | bytes 98312 | tf_op jit(solution)/shard_map/ppermute | solution.py:165
  127.3 16.0 %copy-start.3 = (f32[2,512]{1,0:T(2,128)S(1)}, f32[2,512]{1,0:T(2,128)}, u32[]{:S(2)}) copy-start(f32[2,512]{1,0:T(2,128)} %mix_gain.3) | copy-start | bytes 12292
  143.5 1.4 copy-start.2
